TPU v7x, 32 devices: a whole 2x2x4 slice. The times are simulated.
32 devices in a mesh: sp: 8 (over z, x), tp: 4 (over y, core).
Axes of the slice: x: 2, y: 2, z: 4, core: 2. Of those that a mesh axis runs over, the one named last changes fastest.
Arguments:
- query_wide: bfloat16 [1024, 1536], P('sp', 'tp'), may hold values from -600 to 600
- query_narrow: bfloat16 [1024, 1024], P('sp', 'tp'), may hold values from -600 to 600
- latent: bfloat16 [1024, 512], P('sp'), may hold values from -6 to 6
- rope_key: bfloat16 [1024, 64], P('sp'), may hold values from -6 to 6
- latent_norm_weight: float32 [512], replicated, may hold values from 0.1 to 1.9
- broad_key_lift: bfloat16 [512, 1024], P(None, 'tp'), may hold values from -0.25 to 0.25
- broad_value_lift: bfloat16 [512, 1024], P(None, 'tp'), may hold values from -0.25 to 0.25
- slim_key_lift: bfloat16 [512, 512], P(None, 'tp'), may hold values from -0.25 to 0.25
- slim_value_lift: bfloat16 [512, 512], P(None, 'tp'), may hold values from -0.25 to 0.25
- out_wide: bfloat16 [1024, 2048], P('tp'), may hold values from -0.4375 to 0.4375
- out_narrow: bfloat16 [512, 2048], P('tp'), may hold values from -0.4375 to 0.4375
- resid: bfloat16 [1024, 2048], P('sp'), may hold values from -20 to 20
- ffn_gain: float32 [2048], replicated, may hold values from 0.1 to 1.9
- group_route: int32 [1024], P('sp'), may hold values from 0 to 7, as said below
- expert_pair: int32 [1024, 2], P('sp'), may hold values from 0 to 3, all different within a row
- group_prob: float32 [1024], P('sp'), may hold values from 0.2 to 1
- expert_prob: float32 [1024, 2], P('sp'), may hold values from 0.05 to 1
- gate_weight: bfloat16 [8, 4, 2048, 512], P('sp', None, None, 'tp'), may hold values from -0.125 to 0.125
- up_weight: bfloat16 [8, 4, 2048, 512], P('sp', None, None, 'tp'), may hold values from -0.125 to 0.125
- down_weight: bfloat16 [8, 4, 512, 2048], P('sp', None, 'tp'), may hold values from -0.25 to 0.25
Outputs:
- mixed: bfloat16 [1024, 2048], P('sp', 'tp')
Inputs may be any that keep to these rules, and one draw needn't show every extreme that they name: `group_route`: of the 128 tokens of one index of sp at most 32 name one group; in every draw one group is named by exactly 32 tokens of every index of sp, and every index of sp names one more group exactly 32 times. `expert_pair`: A token's two experts are different.
All inputs are finite; a program needn't handle non-finite values.
Results may differ from a plain program's by a relative error of at most 0.017.
Values may be sent and summed in bfloat16 or wider, within the bound.
A program may use at most 128 MiB of HBM per device.

v0:
```python
import math

import jax
import jax.numpy as jnp
from jax import lax
from jax.sharding import PartitionSpec as P

PLAIN_WIDTH_WIDE = 128
PLAIN_WIDTH_SLIM = 64
ROPE = 64
VALUE_WIDTH_WIDE = 128
VALUE_WIDTH_SLIM = 64
EPG = 4


ROPE_BASE = 10000.0
EPSILON = 1e-06
MASKED = -1e30


def rms_scale(values, gain_row):
    widened = values.astype(jnp.float32)
    return (
        widened
        * lax.rsqrt(jnp.mean(widened * widened, axis=-1, keepdims=True) + EPSILON)
        * gain_row
    )


def angles(positions, width):
    frequency = 1.0 / ROPE_BASE ** (jnp.arange(0, width, 2).astype(jnp.float32) / width)
    return positions.astype(jnp.float32)[:, None] * frequency[None, :]


def rotary(values, angle_table):
    half_width = values.shape[-1] // 2
    first_half = values[..., :half_width]
    second = values[..., half_width:]
    return jnp.concatenate(
        [
            first_half * jnp.cos(angle_table) - second * jnp.sin(angle_table),
            second * jnp.cos(angle_table) + first_half * jnp.sin(angle_table),
        ],
        axis=-1,
    )


def split_query(queries, head_count, nope_width, angle_table):
    shaped = queries.reshape(queries.shape[0], head_count, nope_width + ROPE)
    turned = rotary(shaped[..., nope_width:].astype(jnp.float32), angle_table[:, None, :]).astype(
        jnp.bfloat16
    )
    return (shaped[..., :nope_width], turned)


def group_step(
    carry_state, query_pair, key_block, value_block, rot_block, key_pos, query_pos, scale
):
    row_peak, row_total, accum_out = carry_state
    scores = jnp.einsum(
        "thd,khd->htk", query_pair[0], key_block, preferred_element_type=jnp.float32
    )
    scores = scores + jnp.einsum(
        "thd,kd->htk", query_pair[1], rot_block, preferred_element_type=jnp.float32
    )
    scores = jnp.where((query_pos[:, None] >= key_pos[None, :])[None], scores * scale, MASKED)
    new_peak = jnp.maximum(row_peak, jnp.max(scores, axis=-1))
    keep_factor = jnp.exp(row_peak - new_peak)
    weights = jnp.exp(scores - new_peak[:, :, None])
    row_total = row_total * keep_factor + jnp.sum(weights, axis=-1)
    accum_out = accum_out * keep_factor.T[:, :, None] + jnp.einsum(
        "htk,khd->thd",
        weights.astype(jnp.bfloat16),
        value_block,
        preferred_element_type=jnp.float32,
    )
    return (new_peak, row_total, accum_out)


def empty_state(head_count, width, local_tokens):
    return (
        jnp.full((head_count, local_tokens), MASKED, jnp.float32),
        jnp.zeros((head_count, local_tokens), jnp.float32),
        jnp.zeros((local_tokens, head_count, width), jnp.float32),
    )


def finish(carry_state):
    normalized = carry_state[2] / carry_state[1].T[:, :, None]
    return normalized.astype(jnp.bfloat16).reshape(normalized.shape[0], -1)


def project(latent_rows, weight):
    return jnp.dot(latent_rows, weight, preferred_element_type=jnp.float32).astype(jnp.bfloat16)


def body(
    query_wide,
    query_narrow,
    latent,
    rope_key,
    latent_norm_weight,
    broad_key_lift,
    broad_value_lift,
    slim_key_lift,
    slim_value_lift,
    out_wide,
    out_narrow,
    resid,
    ffn_gain,
    group_route,
    expert_pair,
    group_prob,
    expert_prob,
    gate_weight,
    up_weight,
    down_weight,
):
    local_tokens = latent.shape[0]
    offset = lax.axis_index("sp") * local_tokens
    query_pos = offset + jnp.arange(local_tokens, dtype=jnp.int32)
    angle_table = angles(query_pos, ROPE)
    latent_rows = rms_scale(latent, latent_norm_weight).astype(jnp.bfloat16)
    rot_key = rotary(rope_key.astype(jnp.float32), angle_table).astype(jnp.bfloat16)
    heads_wide = query_wide.shape[1] // (PLAIN_WIDTH_WIDE + ROPE)
    heads_narrow = query_narrow.shape[1] // (PLAIN_WIDTH_SLIM + ROPE)
    wide_query = split_query(query_wide, heads_wide, PLAIN_WIDTH_WIDE, angle_table)
    narrow_query = split_query(query_narrow, heads_narrow, PLAIN_WIDTH_SLIM, angle_table)

    def expand(lat_block):
        return (
            project(lat_block, broad_key_lift),
            project(lat_block, broad_value_lift),
            project(lat_block, slim_key_lift),
            project(lat_block, slim_value_lift),
        )

    def attend(carry_state, key_set, key_pos):
        key_w, value_w, key_n, value_n, rot_block = key_set
        block_rows = rot_block.shape[0]
        wide_state = group_step(
            carry_state[0],
            wide_query,
            key_w.reshape(block_rows, heads_wide, PLAIN_WIDTH_WIDE),
            value_w.reshape(block_rows, heads_wide, VALUE_WIDTH_WIDE),
            rot_block,
            key_pos,
            query_pos,
            (PLAIN_WIDTH_WIDE + ROPE) ** (-0.5),
        )
        narrow_state = group_step(
            carry_state[1],
            narrow_query,
            key_n.reshape(block_rows, heads_narrow, PLAIN_WIDTH_SLIM),
            value_n.reshape(block_rows, heads_narrow, VALUE_WIDTH_SLIM),
            rot_block,
            key_pos,
            query_pos,
            (PLAIN_WIDTH_SLIM + ROPE) ** (-0.5),
        )
        return (wide_state, narrow_state)

    start_state = (
        empty_state(heads_wide, VALUE_WIDTH_WIDE, local_tokens),
        empty_state(heads_narrow, VALUE_WIDTH_SLIM, local_tokens),
    )
    pieces = (
        lax.all_gather(latent_rows, "sp", axis=0, tiled=True),
        lax.all_gather(rot_key, "sp", axis=0, tiled=True),
    )
    total_rows = pieces[0].shape[0]
    block_rows = math.gcd(total_rows, 1024)

    def visit_block(block_index, carry_inner):
        block_start = block_index * block_rows
        sliced = tuple(
            (lax.dynamic_slice_in_dim(piece, block_start, block_rows, 0) for piece in pieces)
        )
        key_pos = block_start + jnp.arange(block_rows, dtype=jnp.int32)

        def work_block(running):
            key_set = expand(sliced[0]) + (sliced[1],)
            return attend(running, key_set, key_pos)

        return lax.cond(
            block_start > query_pos[-1], lambda unchanged: unchanged, work_block, carry_inner
        )

    final_state = lax.fori_loop(0, total_rows // block_rows, visit_block, start_state)
    att_wide = finish(final_state[0])
    att_narrow = finish(final_state[1])
    partial_value = jnp.dot(att_wide, out_wide, preferred_element_type=jnp.float32)
    partial_value = partial_value + jnp.dot(
        att_narrow, out_narrow, preferred_element_type=jnp.float32
    )
    model_width = resid.shape[1]
    tp_size = lax.axis_size("tp")
    quarter = model_width // tp_size
    col_start = lax.axis_index("tp") * quarter
    summed = lax.psum(partial_value.astype(jnp.bfloat16), "tp").astype(jnp.float32)
    stream = (resid.astype(jnp.float32) + summed).astype(jnp.bfloat16)
    normed = rms_scale(stream, ffn_gain).astype(jnp.bfloat16)
    stream_cols = lax.dynamic_slice_in_dim(stream, col_start, quarter, 1)
    groups = lax.axis_size("sp")
    capacity = 2 * local_tokens // groups
    share_of = group_prob[:, None] * expert_prob / jnp.sum(expert_prob, axis=1, keepdims=True)
    chosen = (expert_pair[:, :, None] == jnp.arange(EPG, dtype=jnp.int32)[None, None, :]).astype(
        jnp.float32
    )
    combine = jnp.sum(share_of[:, :, None] * chosen, axis=1).astype(jnp.bfloat16)
    member = (group_route[:, None] == jnp.arange(groups, dtype=jnp.int32)[None, :]).astype(
        jnp.int32
    )
    group_rank = jnp.sum(jnp.cumsum(member, axis=0) * member, axis=1) - 1
    slot_index = group_route * capacity + group_rank
    routed_weights = jnp.zeros((groups * capacity, EPG), jnp.bfloat16).at[slot_index].set(combine)
    routed_weights = routed_weights.reshape(groups, capacity, EPG)
    column_rows = lax.dynamic_slice_in_dim(normed, col_start, quarter, 1)
    placed = (
        jnp.zeros((groups * capacity, column_rows.shape[1]), jnp.bfloat16)
        .at[slot_index]
        .set(column_rows)
    )
    joined = lax.all_gather(
        lax.all_to_all(
            placed.reshape(groups, capacity, column_rows.shape[1]),
            "sp",
            split_axis=0,
            concat_axis=0,
            tiled=True,
        ),
        "tp",
        axis=2,
        tiled=True,
    )
    slot_count = joined.shape[0] * joined.shape[1]
    flat_rows = joined.reshape(slot_count, joined.shape[2])
    gate_act = jnp.einsum(
        "rd,edf->ref", flat_rows, gate_weight[0], preferred_element_type=jnp.float32
    )
    up_act = jnp.einsum("rd,edf->ref", flat_rows, up_weight[0], preferred_element_type=jnp.float32)
    scaled = (
        lax.all_to_all(routed_weights, "sp", split_axis=0, concat_axis=0, tiled=True)
        .reshape(slot_count, EPG)
        .astype(jnp.float32)[:, :, None]
    )
    hidden = (jax.nn.silu(gate_act) * up_act * scaled).astype(jnp.bfloat16)
    partials = jnp.einsum("ref,efd->rd", hidden, down_weight[0], preferred_element_type=jnp.float32)
    partials = partials.reshape(joined.shape)
    summed_rows = lax.psum_scatter(
        partials.astype(jnp.bfloat16), "tp", scatter_dimension=2, tiled=True
    )
    returned_rows = lax.all_to_all(summed_rows, "sp", split_axis=0, concat_axis=0, tiled=True)
    moe_rows = returned_rows.reshape(groups * capacity, quarter)[slot_index]
    return (stream_cols.astype(jnp.float32) + moe_rows.astype(jnp.float32)).astype(jnp.bfloat16)


def solution(mesh):
    placed = (
        P("sp", "tp"),
        P("sp", "tp"),
        P("sp", None),
        P("sp", None),
        P(),
        P(None, "tp"),
        P(None, "tp"),
        P(None, "tp"),
        P(None, "tp"),
        P("tp", None),
        P("tp", None),
        P("sp", None),
        P(),
        P("sp"),
        P("sp", None),
        P("sp"),
        P("sp", None),
        P("sp", None, None, "tp"),
        P("sp", None, None, "tp"),
        P("sp", None, "tp", None),
    )
    return jax.shard_map(body, mesh=mesh, in_specs=placed, out_specs=P("sp", "tp"), check_vma=False)
```

profile of v0, /device:TPU:0, one launch (start us, length us, event | category | flops | bytes accessed | tf_op | source)
XLA Modules:
  0.0 180.7 jit_solution(8999266724435186518)
XLA Ops:
  6.5 1.2 fusion.38
  7.7 1.7 fusion.40
  9.5 0.7 convert_element_type.130
  10.2 1.0 copy.74
  11.2 1.0 copy.75
  12.2 0.6 slice.38
  13.5 0.7 fusion.48
  14.6 28.3 %all_gather.10 = bf16[1024,64]{0,1:T(8,128)(2,1)S(1)} all-gather(bf16[128,64]{0,1:T(8,128)(2,1)S(1)} %pad_maximum_fusion.2), channel_id=1, replica_groups=mesh['sp'=8,'tp'=4] {'sp'}, dimensions={0}, use_global_device_ids=true | all-gather | bytes 147456 | tf_op jit(solution)/shard_map/all_gather | solution.py:169
  43.0 0.6 pad_maximum_fusion
  43.6 9.6 %all-gather.3.cloned.1.call-done = bf16[1024,512]{1,0:T(8,128)(2,1)} async-done(((bf16[128,512]{1,0:T(8,128)(2,1)}), bf16[1024,512]{1,0:T(8,128)(2,1)}) %all-gather.3.cloned.1.call-update) | async-done | bytes 1048592 | tf_op jit(solution)/shard_map/all_gather | solution.py:168
  53.2 7.1 %conditional.1 = (f32[2,128]{1,0:T(2,128)S(1)}, f32[128,2,128]{0,2,1:T(8,128)S(1)}, f32[2,128]{1,0:T(2,128)S(1)}, f32[128,2,64]{0,2,1:T(8,128)S(1)}) conditional(s32[]{:T(128)} %bitcast.13, (s32[128]{0:T(128)S(1)}, s32[1024]{0:T(1024)S(1)}, bf16[1024,512]{1,0:T(8,128)(2,1)}, bf16[512,256]{1,0:T(8,128)(2,1)S(1)}, bf16[128,2,192]{0,2,1:T(8,128)(2,1)S(1)}, ...), branch_computations={%region_1.6_spmd, %region_6.7_spmd} | conditional | flops 1078953472 | bytes 26996452 | solution.py:185
  53.2 0.6 copy-done.6
  53.8 1.7 convolution_convert_fusion.1
  60.4 1.6 fusion.54
  62.0 1.1 fusion.23
  63.4 0.8 dynamic-slice
  64.2 31.1 %all-reduce.2.cloned.1.call-done = bf16[128,2048]{1,0:T(8,128)(2,1)} async-done(((bf16[128,2048]{1,0:T(8,128)(2,1)}), bf16[128,2048]{1,0:T(8,128)(2,1)}) %all-reduce.2.cloned.1.call-update) | async-done | bytes 524304 | tf_op jit(solution)/shard_map/psum | solution.py:200
  95.3 1.3 multiply_reduce_fusion
  96.6 1.1 convert_element_type.142
  97.7 1.6 scatter_custom_fusion
  99.3 13.6 %all_to_all.15 = bf16[8,32,512]{2,1,0:T(8,128)(2,1)} all-to-all(bf16[8,32,512]{2,1,0:T(8,128)(2,1)S(1)} %bitcast.107), channel_id=1, replica_groups=mesh['sp'=8,'tp'=4] {'sp'}, dimensions={0} | all-to-all | bytes 524288 | tf_op jit(solution)/shard_map/all_to_all | solution.py:225
  113.2 0.9 scatter_custom_fusion.1
  114.2 9.7 %all_to_all.16 = bf16[8,32,4]{1,2,0:T(4,128)(2,1)S(1)} all-to-all(bf16[8,32,4]{1,2,0:T(4,128)(2,1)S(1)} %copy.78), channel_id=1, replica_groups=mesh['sp'=8,'tp'=4] {'sp'}, dimensions={0} | all-to-all | bytes 4096 | tf_op jit(solution)/shard_map/all_to_all | solution.py:243
  124.0 4.1 %all-gather.5.cloned.1.call-done = bf16[8,32,2048]{2,1,0:T(8,128)(2,1)} async-done(((bf16[8,32,512]{2,1,0:T(8,128)(2,1)}), bf16[8,32,2048]{2,1,0:T(8,128)(2,1)}) %all-gather.5.cloned.1.call-update) | async-done | bytes 1048592 | tf_op jit(solution)/shard_map/all_gather | solution.py:224
  128.1 2.8 %fusion.27 = f32[256,4,128]{2,0,1:T(8,128)S(1)} fusion(bf16[256,2048,1]{1,0,2:T(8,128)(2,1)} %bitcast.119, bf16[1,4,2048,128]{3,2,1,0:T(8,128)(2,1)} %param.39), kind=kOutput, calls=%fused_computation.49 | convolution fusion | flops 536870912 | bytes 3670016 | tf_op jit(solution)/shard_map/rd,edf->ref/dot_general | solution.py:238
  130.9 0.7 fusion.35
  131.7 1.7 fusion.22
  133.4 24.9 %reduce-scatter.2.cloned.1.call-done = bf16[8,32,512]{2,1,0:T(8,128)(2,1)} async-done(((bf16[8,32,2048]{2,1,0:T(8,128)(2,1)}), bf16[8,32,512]{2,1,0:T(8,128)(2,1)}) %reduce-scatter.2.cloned.1.call-update) | async-done | bytes 262160 | tf_op jit(solution)/shard_map/reduce_scatter | solution.py:250
  158.3 5.5 %all-to-all-start.2 = ((bf16[8,32,512]{2,1,0:T(8,128)(2,1)}), bf16[8,32,512]{2,1,0:T(8,128)(2,1)S(1)}, u32[]{:S(2)}, u32[]{:S(2)}) async-start(bf16[8,32,512]{2,1,0:T(8,128)(2,1)} %reduce-scatter.2.cloned.1.call-done), calls=%async_computation.3 | async-start | bytes 524288 | tf_op jit(solution)/shard_map/all_to_all | solution.py:253
  163.9 8.7 %all-to-all-done.2 = bf16[8,32,512]{2,1,0:T(8,128)(2,1)S(1)} async-done(((bf16[8,32,512]{2,1,0:T(8,128)(2,1)}), bf16[8,32,512]{2,1,0:T(8,128)(2,1)S(1)}, u32[]{:S(2)}, u32[]{:S(2)}) %all-to-all-start.2) | async-done | bytes 262176 | tf_op jit(solution)/shard_map/all_to_all | solution.py:253
  172.6 0.8 gather_fusion
  173.4 0.7 add_convert_fusion.1
  (83 shorter events, 5.9 us)
Async XLA Ops:
  6.5 125.1 %copy-start = (bf16[1,4,128,2048]{3,2,1,0:T(8,128)(2,1)S(1)}, bf16[1,4,128,2048]{3,2,1,0:T(8,128)(2,1)}, u32[]{:S(2)}) copy-start(bf16[1,4,128,2048]{3,2,1,0:T(8,128)(2,1)} %param.41) | copy-start | bytes 6291460
  6.5 46.6 %copy-start.4 = (bf16[512,256]{1,0:T(8,128)(2,1)S(1)}, bf16[512,256]{1,0:T(8,128)(2,1)}, u32[]{:S(2)}) copy-start(bf16[512,256]{1,0:T(8,128)(2,1)} %param.27) | copy-start | bytes 786436
  6.5 46.6 %all-gather.3.cloned.1.call-start = ((), (), s32[]{:S(2)}) async-start(), calls=%async_computation.4 | async-start | bytes 1179648 | tf_op jit(solution)/shard_map/all_gather | solution.py:168
  9.4 85.8 %all-reduce.2.cloned.1.call-start = ((), (), s32[]{:S(2)}) async-start(), calls=%async_computation.5 | async-start | bytes 1048576 | tf_op jit(solution)/shard_map/psum | solution.py:200
  53.2 0.6 copy-start.6
  55.6 1.2 copy-start.1
  55.6 1.2 copy-start.9
  56.0 1.3 copy-start.7
  56.2 1.5 copy-start.8
  57.7 0.9 copy-start.10
  58.1 1.3 copy-start.5
  60.3 1.7 copy-start.3
  60.4 2.9 %copy-start.12 = (s32[128]{0:T(128)S(1)}, s32[128]{0:T(128)}, u32[]{:S(2)}) copy-start(s32[128]{0:T(128)} %param.35) | copy-start | bytes 1540
  60.4 34.9 %copy-start.2 = (bf16[128,2048]{1,0:T(8,128)(2,1)S(1)}, bf16[128,2048]{1,0:T(8,128)(2,1)}, u32[]{:S(2)}) copy-start(bf16[128,2048]{1,0:T(8,128)(2,1)} %param.33) | copy-start | bytes 1572868
  63.2 64.9 %all-gather.5.cloned.1.call-start = ((), (), s32[]{:S(2)}) async-start(), calls=%async_computation.6 | async-start | bytes 1310720 | tf_op jit(solution)/shard_map/all_gather | solution.py:224
  64.2 48.8 %copy-start.11 = (f32[128,2]{0,1:T(2,128)S(1)}, f32[128,2]{0,1:T(2,128)}, u32[]{:S(2)}) copy-start(f32[128,2]{0,1:T(2,128)} %param.38) | copy-start | bytes 3076
  64.2 48.8 %copy-start.14 = (f32[128]{0:T(128)S(1)}, f32[128]{0:T(128)}, u32[]{:S(2)}) copy-start(f32[128]{0:T(128)} %param.37) | copy-start | bytes 1540
  64.2 48.9 %copy-start.13 = (s32[128,2]{0,1:T(2,128)S(1)}, s32[128,2]{0,1:T(2,128)}, u32[]{:S(2)}) copy-start(s32[128,2]{0,1:T(2,128)} %param.36) | copy-start | bytes 3076
  112.9 45.4 %reduce-scatter.2.cloned.1.call-start = ((), (), s32[]{:S(2)}) async-start(), calls=%async_computation.7 | async-start | bytes 1310720 | tf_op jit(solution)/shard_map/reduce_scatter | solution.py:250
  128.1 2.8 %copy-start.15 = (bf16[1,4,2048,128]{3,2,1,0:T(8,128)(2,1)S(1)}, bf16[1,4,2048,128]{3,2,1,0:T(8,128)(2,1)}, u32[]{:S(2)}) copy-start(bf16[1,4,2048,128]{3,2,1,0:T(8,128)(2,1)} %param.40) | copy-start | bytes 6291460
  128.1 2.8 %copy-start.16 = (bf16[8,32,2048]{2,1,0:T(8,128)(2,1)S(1)}, bf16[8,32,2048]{2,1,0:T(8,128)(2,1)}, u32[]{:S(2)}) copy-start(bf16[8,32,2048]{2,1,0:T(8,128)(2,1)} %all-gather.5.cloned.1.call-done) | copy-start | bytes 3145732
  158.3 14.3 %all-to-all-start.2 = ((bf16[8,32,512]{2,1,0:T(8,128)(2,1)}), bf16[8,32,512]{2,1,0:T(8,128)(2,1)S(1)}, u32[]{:S(2)}, u32[]{:S(2)}) async-start(bf16[8,32,512]{2,1,0:T(8,128)(2,1)} %reduce-scatter.2.cloned.1.call-done), calls=%async_computation.3 | async-start | bytes 524288 | tf_op jit(solution)/shard_map/all_to_all | solution.py:253
Sparse Core Ops, SparseCore 0:
  9.5 43.5 all-gather.2
  63.3 31.9 all-reduce.1
  113.1 14.9 all-gather.4
  133.5 24.7 reduce-scatter.1
where the time goes:
time: 181 us
  waiting for transfers between devices  78.5 us (43%)
  blocking collectives  51.6 us (29%)
  between operations  14 us (8%)
  matrix products  13.2 us (7%)
  other arithmetic  10.8 us (6%)
  local copies, waits for them, and re-layouts  6.7 us (4%)
  starting transfers between devices  5.64 us (3%)
    psum x1, waiting for transfers between devices, body(): lax.psum(partial_value.astype(jnp.bfloat16), 'tp').astype(jnp.float32)  31.1 us
    all_gather x1, blocking collectives, body(): lax.all_gather(rot_key, 'sp', axis=0, tiled=True)  28.3 us
    reduce_scatter x1, waiting for transfers between devices, body(): lax.psum_scatter(partials.astype(jnp.bfloat16), 'tp', scatter_dimension=2...  24.9 us
    all_to_all x1, blocking collectives, body(): lax.all_to_all(placed.reshape(groups, capacity, column_rows.shape[1]), 's...  13.6 us
    all_to_all x1, blocking collectives, body(): lax.all_to_all(routed_weights, 'sp', split_axis=0, concat_axis=0, tiled=T...  9.66 us
    all_gather x1, waiting for transfers between devices, body(): lax.all_gather(latent_rows, 'sp', axis=0, tiled=True)  9.58 us
    all_to_all x1, waiting for transfers between devices, body(): lax.all_to_all(summed_rows, 'sp', split_axis=0, concat_axis=0, tiled=True)  8.74 us
    all_to_all x1, starting transfers between devices, body(): lax.all_to_all(summed_rows, 'sp', split_axis=0, concat_axis=0, tiled=True)  5.51 us
  transfers between devices with their start and end apart: 5, of which 5 were waited for; matrix products, arithmetic and copies ran while one was open for 4% of the time, Pallas kernels for 0%

commit v1 on v0

v1 whole, which is shorter than its diff:
```python
import functools

import jax
import jax.numpy as jnp
import numpy as np
from jax import lax
from jax.experimental import pallas as pl
from jax.experimental.pallas import tpu as pltpu
from jax.sharding import PartitionSpec as P

PLAIN_WIDE = 128
PLAIN_SLIM = 64
ROPE = 64
LANES = 128
ROPE_BASE = 10000.0
EPSILON = 1e-06
MASKED = -1e30
F32 = jnp.float32
BF16 = jnp.bfloat16
MESH = pl.DeviceIdType.MESH


def dot(a, b):
    return jnp.dot(a, b, preferred_element_type=F32)


def dot_nt(a, b):
    return lax.dot_general(a, b, (((1,), (1,)), ((), ())), preferred_element_type=F32)


def dot_tn(a, b):
    return lax.dot_general(a, b, (((0,), (0,)), ((), ())), preferred_element_type=F32)


def loop(lo, hi, fn):
    def step(i, carry):
        fn(i)
        return carry

    lax.fori_loop(lo, hi, step, 0)


def kernel(
    n_sp, n_tp, cap,
    qw_h, qn_h, lat_h, rk_h, lnw, bk_h, bv_h, sk_h, sv_h, ow_h, on_h, res_h, gain, meta,
    base_t, local_t, gate_h, up_h, down_h,
    out_ref,
    qw, qn, lat, rk, lift, wout, res, gu, down,
    own_lat, lat_all, kbuf, vbuf, att, part, part_in, xs, cs, rx, comb, nx, hid, pd, d1, e1, d2, fin, ret,
    ld_sem, snd, rcv_a, rcv_b, snd_b, rcv_k, snd_k, rcv_c, snd_d, rcv_d1, rcv_d2, rcv_g,
):
    me = lax.axis_index("sp")
    j = lax.axis_index("tp")
    j2 = lax.rem(j + 2, 4)
    j1 = j + 1 - 2 * lax.rem(j, 2)
    j3 = lax.rem(j1 + 2, 4)
    rel = (j, j1, j2, j3)
    tok = lat.shape[0]
    rank = lat.shape[1]
    quarter = res.shape[1]
    experts = gu.shape[0]
    ff = gu.shape[2] // 2
    slots = n_sp * cap
    kw = bk_h.shape[1]
    kn = sk_h.shape[1]
    heads_w = kw // PLAIN_WIDE
    heads_n = kn // PLAIN_SLIM
    piece = tok // n_tp

    barrier = pltpu.get_barrier_semaphore()

    def greet(i):
        pl.semaphore_signal(barrier, inc=1, device_id=(lax.rem(me + i, n_sp), j), device_id_type=MESH)

    loop(1, n_sp, greet)
    for r in (1, 2, 3):
        pl.semaphore_signal(barrier, inc=1, device_id=(me, rel[r]), device_id_type=MESH)

    loads = []

    def load(src, dst):
        c = pltpu.make_async_copy(src, dst, ld_sem.at[len(loads)])
        c.start()
        loads.append(c)
        return c

    first = [load(lat_h, lat), load(rk_h, rk)]
    queries = [load(qw_h, qw), load(qn_h, qn)]
    lifts = [
        load(bk_h, lift.at[:, pl.ds(0, kw)]),
        load(bv_h, lift.at[:, pl.ds(kw, kw)]),
        load(sk_h, lift.at[:, pl.ds(2 * kw, kn)]),
        load(sv_h, lift.at[:, pl.ds(2 * kw + kn, kn)]),
    ]
    outs = [
        load(ow_h, wout.at[pl.ds(0, kw)]),
        load(on_h, wout.at[pl.ds(kw, kn)]),
        load(res_h.at[:, pl.ds(pl.multiple_of(j * quarter, quarter), quarter)], res),
    ]
    weights = [
        load(gate_h.at[0], gu.at[:, :, pl.ds(0, ff)]),
        load(up_h.at[0], gu.at[:, :, pl.ds(ff, ff)]),
    ]
    for e in range(experts):
        weights.append(load(down_h.at[0, e], down.at[pl.ds(e * ff, ff)]))

    lane = lax.broadcasted_iota(jnp.int32, (tok, LANES), 1)
    low = lane < 64
    cb = base_t[0, pl.ds(me, 1), :]
    sb = base_t[1, pl.ds(me, 1), :]
    cl = local_t[0]
    sl = local_t[1]
    cos = cb * cl - sb * sl
    sin = sb * cl + cb * sl
    first_half = lax.rem(lane, 64) < 32
    sin = jnp.where(first_half, -sin, sin)
    ones = jnp.ones_like(cos)
    zeros = jnp.zeros_like(cos)

    def turn(x, c, s):
        swapped = jnp.where(first_half, pltpu.roll(x, 96, 1), pltpu.roll(x, 32, 1))
        return x * c + swapped * s

    for c in first:
        c.wait()
    dup = (lax.broadcasted_iota(jnp.int32, (ROPE, LANES), 0)
           == lax.rem(lax.broadcasted_iota(jnp.int32, (ROPE, LANES), 1), 64)).astype(BF16)
    rk2 = turn(dot(rk[...], dup), cos, sin).astype(BF16)
    x = lat[...].astype(F32)
    rows = (x * lax.rsqrt(jnp.mean(x * x, axis=-1, keepdims=True) + EPSILON) * lnw[...]).astype(BF16)
    own_lat[:, :, 0:rank] = rows.reshape(n_tp, piece, rank)
    own_lat[:, :, rank:] = rk2.reshape(n_tp, piece, LANES)
    lat_all[pl.ds(me, 1), :, :, 0:rank] = rows.reshape(1, n_tp, piece, rank)
    lat_all[pl.ds(me, 1), :, :, rank:] = rk2.reshape(1, n_tp, piece, LANES)

    pl.semaphore_wait(barrier, n_sp - 1 + 3)

    def copy(src, dst, s_sem, r_sem, dev):
        return pltpu.make_async_remote_copy(
            src_ref=src, dst_ref=dst, send_sem=s_sem, recv_sem=r_sem, device_id=dev, device_id_type=MESH
        )

    def lat_sp(dest):
        return copy(own_lat.at[j], lat_all.at[me, j], snd.at[dest, 0], rcv_a.at[me, 0], (dest, j))

    loop(me + 1, n_sp, lambda d: lat_sp(d).start())

    meta_v = meta[...]
    route = meta_v[0:1, :]
    gcol = lax.broadcasted_iota(jnp.int32, (max(n_sp, 8), tok), 0).astype(F32)
    member = (gcol == route).astype(F32)
    upper = (lax.broadcasted_iota(jnp.int32, (tok, tok), 0)
             <= lax.broadcasted_iota(jnp.int32, (tok, tok), 1)).astype(BF16)
    ranks = dot(member.astype(BF16), upper)
    rank_row = jnp.sum(member * ranks, axis=0, keepdims=True) - 1.0
    slot_row = route * float(cap) + rank_row
    slot_iota = lax.broadcasted_iota(jnp.int32, (slots, tok), 0).astype(F32)
    place = (slot_iota == slot_row).astype(BF16)
    eiota = lax.broadcasted_iota(jnp.int32, (LANES, tok), 0).astype(F32)
    total = meta_v[4:5, :] + meta_v[5:6, :]
    combine = jnp.zeros((LANES, tok), F32)
    for k in range(2):
        share = meta_v[3:4, :] * meta_v[4 + k:5 + k, :] / total
        combine = combine + jnp.where(eiota == meta_v[1 + k:2 + k, :], share, 0.0)
    cs_v = dot_nt(place, combine.astype(BF16)).astype(BF16).reshape(n_sp, cap, LANES)
    cs[...] = cs_v

    for c in queries:
        c.wait()

    def tile(ref, k):
        return ref[:, k * LANES:(k + 1) * LANES].astype(F32)

    cos_a, sin_a = jnp.where(low, cos, ones), jnp.where(low, sin, zeros)
    cos_b, sin_b = jnp.where(low, ones, cos), jnp.where(low, zeros, sin)
    q_wide = []
    for h in range(heads_w):
        start = h * (PLAIN_WIDE + ROPE)
        if start % LANES == 0:
            k = start // LANES
            nope = tile(qw, k)
            rot = turn(tile(qw, k + 1), cos_a, sin_a)
        else:
            k = start // LANES
            t1 = pltpu.roll(tile(qw, k), 64, 1)
            t2 = pltpu.roll(tile(qw, k + 1), 64, 1)
            nope = jnp.where(low, t1, t2)
            rot = turn(t2, cos_a, sin_a)
        q_wide.append(jnp.concatenate(
            [nope.astype(BF16), jnp.where(low, rot, zeros).astype(BF16)], axis=1))
    q_slim = []
    for h in range(heads_n):
        y = turn(tile(qn, h), cos_b, sin_b)
        if h % 2 == 1:
            y = pltpu.roll(y, 64, 1)
        q_slim.append(y.astype(BF16))

    kbuf[...] = jnp.zeros_like(kbuf)
    vbuf[...] = jnp.zeros_like(vbuf)

    def comb_sp(dest):
        return copy(cs.at[dest], comb.at[me], snd_k.at[dest], rcv_k.at[me], (dest, j))

    def others(fn):
        loop(1, n_sp, lambda i: fn(lax.rem(me + i, n_sp)))

    others(lambda d: comb_sp(d).start())
    comb[pl.ds(me, 1)] = dot_nt(
        (lax.broadcasted_iota(jnp.int32, (cap, tok), 0).astype(F32) + (me * cap).astype(F32)
         == slot_row).astype(BF16), combine.astype(BF16)).astype(BF16)[None]

    def gather(buf, s, r, rcv):
        if r == 2:
            return copy(buf.at[s, j], buf.at[s, j], snd.at[s, 1], rcv.at[s, 2], (me, j2))
        if r == 1:
            return copy(buf.at[s, j], buf.at[s, j], snd.at[s, 2], rcv.at[s, 1], (me, j1))
        return copy(buf.at[s, j2], buf.at[s, j2], snd.at[s, 3], rcv.at[s, 3], (me, j1))

    def arrived(buf, s, r, rcv):
        copy(buf.at[s, rel[r]], buf.at[s, rel[r]], snd.at[s, 0], rcv.at[s, r], (me, j1)).wait_recv()

    for c in lifts:
        c.wait()

    def expand(s):
        rows_s = lat_all[pl.ds(s, 1)].reshape(tok, rank + LANES)
        kv = dot(rows_s[:, 0:rank], lift[...]).astype(BF16)
        rot = rows_s[:, rank:]
        at = pl.ds(pl.multiple_of(s * tok, tok), tok)
        for h in range(heads_w):
            kbuf[at, h * 256:h * 256 + 128] = kv[:, h * 128:(h + 1) * 128]
            kbuf[at, h * 256 + 128:(h + 1) * 256] = rot
        vbuf[at, 0:kw] = kv[:, kw:2 * kw]
        off = heads_w * 256
        for h in range(heads_n):
            pair = kv[:, 2 * kw + (h // 2) * 128:2 * kw + (h // 2 + 1) * 128]
            mixed = jnp.where(low, pair, rot) if h % 2 == 0 else jnp.where(low, rot, pair)
            kbuf[at, off + h * 128:off + (h + 1) * 128] = mixed
        vbuf[at, kw:] = kv[:, 2 * kw + kn:]

    def a1(i):
        s = me - 1 - i
        arrived(lat_all, s, 0, rcv_a)
        gather(lat_all, s, 2, rcv_a).start()
        gather(lat_all, s, 1, rcv_a).start()

    def a2(i):
        s = me - 1 - i
        arrived(lat_all, s, 2, rcv_a)
        gather(lat_all, s, 3, rcv_a).start()

    def a3(i):
        s = me - 1 - i
        arrived(lat_all, s, 1, rcv_a)
        arrived(lat_all, s, 3, rcv_a)
        expand(s)

    expand(me)
    loop(0, me, a1)
    loop(0, me, a2)
    loop(0, me, a3)

    keys = n_sp * tok
    chunk = min(keys, 1024)
    n_chunk = keys // chunk

    def head(q, kcol, kwid, vcol, scale):
        def scores(c):
            at = pl.ds(pl.multiple_of(c * chunk, chunk), chunk)
            sc = dot_nt(q, kbuf[at, kcol:kcol + kwid]) * scale
            kpos = c * chunk + lax.broadcasted_iota(jnp.int32, (tok, chunk), 1)
            qpos = me * tok + lax.broadcasted_iota(jnp.int32, (tok, chunk), 0)
            return jnp.where(kpos <= qpos, sc, MASKED), vbuf[at, vcol:vcol + LANES]

        if n_chunk == 1:
            sc, v = scores(0)
            p = jnp.exp(sc - jnp.max(sc, axis=-1, keepdims=True))
            return dot(p.astype(BF16), v) / jnp.sum(p, axis=-1, keepdims=True)

        def step(c, carry):
            m, l, acc = carry
            sc, v = scores(c)
            m2 = jnp.maximum(m, jnp.max(sc, axis=-1, keepdims=True))
            keep = jnp.exp(m - m2)
            p = jnp.exp(sc - m2)
            return m2, l * keep + jnp.sum(p, axis=-1, keepdims=True), acc * keep + dot(p.astype(BF16), v)

        init = (jnp.full((tok, 1), MASKED, F32), jnp.zeros((tok, 1), F32), jnp.zeros((tok, LANES), F32))
        m, l, acc = lax.fori_loop(0, n_chunk, step, init)
        return acc / l

    for h in range(heads_w):
        o = head(q_wide[h], h * 256, 256, h * 128, (PLAIN_WIDE + ROPE) ** -0.5)
        att[:, h * 128:(h + 1) * 128] = o.astype(BF16)
    off = heads_w * 256
    for h in range(0, heads_n, 2):
        o0 = head(q_slim[h], off + h * 128, 128, kw + (h // 2) * 128, (PLAIN_SLIM + ROPE) ** -0.5)
        o1 = head(q_slim[h + 1], off + (h + 1) * 128, 128, kw + (h // 2) * 128, (PLAIN_SLIM + ROPE) ** -0.5)
        att[:, kw + (h // 2) * 128:kw + (h // 2 + 1) * 128] = jnp.where(low, o0, o1).astype(BF16)

    for c in outs:
        c.wait()

    def swap_b(r):
        return copy(part.at[r], part_in.at[r - 1], snd_b.at[r - 1], rcv_b.at[r - 1], (me, rel[r]))

    for r in (2, 3, 1, 0):
        cols = pl.ds(pl.multiple_of(rel[r] * quarter, quarter), quarter)
        y = dot(att[...], wout[:, cols])
        if r == 0:
            mine = y.astype(BF16).astype(F32)
        else:
            part[r] = y.astype(BF16)
            swap_b(r).start()

    loop(me + 1, n_sp, lambda d: lat_sp(d).wait_send())

    def a_done(s):
        for r in (1, 2, 3):
            gather(lat_all, s, r, rcv_a).wait_send()

    loop(0, me, a_done)

    for r in (1, 2, 3):
        swap_b(r).wait_recv()
        mine = mine + part_in[r - 1].astype(F32)
    stream = (res[...].astype(F32) + mine).astype(BF16)

    xs[...] = dot(place, stream).astype(BF16).reshape(n_sp, cap, quarter)
    own_rows = (lax.broadcasted_iota(jnp.int32, (cap, tok), 0).astype(F32) + (me * cap).astype(F32)
                == slot_row).astype(BF16)
    rx[pl.ds(me, 1), pl.ds(j, 1)] = dot(own_rows, stream).astype(BF16)[None, None]

    def rows_sp(dest):
        return copy(xs.at[dest], rx.at[me, j], snd.at[dest, 0], rcv_c.at[me, 0], (dest, j))

    others(lambda d: rows_sp(d).start())

    def c1(s):
        gather(rx, s, 2, rcv_c).start()
        gather(rx, s, 1, rcv_c).start()

    c1(me)

    def c1w(s):
        arrived(rx, s, 0, rcv_c)
        c1(s)

    def c2(s):
        arrived(rx, s, 2, rcv_c)
        gather(rx, s, 3, rcv_c).start()

    def c3(s):
        arrived(rx, s, 1, rcv_c)
        arrived(rx, s, 3, rcv_c)

    others(c1w)
    c2(me)
    others(c2)
    for c in weights:
        c.wait()
    others(lambda s: copy(cs.at[s], comb.at[s], snd_k.at[s], rcv_k.at[s], (s, j)).wait_recv())
    c3(me)
    others(c3)

    blk = min(slots, 256)
    per = blk // cap
    for b in range(slots // blk):
        sq = jnp.zeros((blk, 1), F32)
        for q in range(n_tp):
            v = rx[b * per:(b + 1) * per, q].reshape(blk, quarter).astype(F32)
            sq = sq + jnp.sum(v * v, axis=-1, keepdims=True)
        inv = lax.rsqrt(sq / (n_tp * quarter) + EPSILON)
        for q in range(n_tp):
            v = rx[b * per:(b + 1) * per, q].reshape(blk, quarter).astype(F32)
            nx[:, q * quarter:(q + 1) * quarter] = (v * inv * gain[:, q * quarter:(q + 1) * quarter]).astype(BF16)
        w = comb[b * per:(b + 1) * per].reshape(blk, LANES).astype(F32)
        for e in range(experts):
            y = dot(nx[...], gu[e])
            g, u = y[:, 0:ff], y[:, ff:]
            hid[b * blk:(b + 1) * blk, e * ff:(e + 1) * ff] = (
                g / (1.0 + jnp.exp(-g)) * u * w[:, e:e + 1]).astype(BF16)

    def swap_d(i):
        return copy(pd.at[3 if i else 1], d1.at[i], snd_d.at[i], rcv_d1.at[i], (me, j1))

    for r in (3, 1, 2, 0):
        cols = pl.ds(pl.multiple_of(rel[r] * quarter, quarter), quarter)
        for b in range(slots // blk):
            y = dot(hid[b * blk:(b + 1) * blk], down[:, cols]).astype(BF16)
            pd[r, b * per:(b + 1) * per] = y.reshape(per, cap, quarter)
        if r == 3:
            swap_d(1).start()
        if r == 1:
            swap_d(0).start()

    others(lambda d: rows_sp(d).wait_send())

    def c_done(s):
        for r in (1, 2, 3):
            gather(rx, s, r, rcv_c).wait_send()

    c_done(me)
    others(c_done)
    others(lambda d: comb_sp(d).wait_send())

    def pair_d(s):
        return copy(e1.at[s], d2.at[s], snd.at[s, 0], rcv_d2.at[s], (me, j2))

    def home(s):
        return copy(fin.at[s], ret.at[me], snd.at[s, 1], rcv_g.at[me], (s, j))

    swap_d(1).wait_recv()

    def d_pair(s):
        at = pl.ds(s, 1)
        e1[at] = (pd[2, at].astype(F32) + d1[1, at].astype(F32)).astype(BF16)
        pair_d(s).start()

    others(d_pair)
    d_pair(me)
    swap_d(0).wait_recv()

    def summed(s):
        at = pl.ds(s, 1)
        pair_d(s).wait_recv()
        return (pd[0, at].astype(F32) + d1[0, at].astype(F32) + d2[at].astype(F32)).astype(BF16)

    def d_home(s):
        fin[pl.ds(s, 1)] = summed(s)
        home(s).start()

    others(d_home)
    ret[pl.ds(me, 1)] = summed(me)
    others(lambda s: copy(fin.at[s], ret.at[s], snd.at[s, 1], rcv_g.at[s], (s, j)).wait_recv())
    moe = dot_tn(place, ret[...].reshape(slots, quarter))
    out_ref[...] = (stream.astype(F32) + moe).astype(BF16)

    for r in (1, 2, 3):
        swap_b(r).wait_send()
    swap_d(0).wait_send()
    swap_d(1).wait_send()
    pair_d(me).wait_send()

    def tail(s):
        pair_d(s).wait_send()
        home(s).wait_send()

    others(tail)


def body(
    n_sp, n_tp,
    query_wide, query_narrow, latent, rope_key, latent_norm_weight, broad_key_lift, broad_value_lift,
    slim_key_lift, slim_value_lift, out_wide, out_narrow, resid, ffn_gain, group_route, expert_pair,
    group_prob, expert_prob, gate_weight, up_weight, down_weight,
):
    tok, rank = latent.shape
    width = resid.shape[1]
    quarter = width // n_tp
    experts, _, ff = gate_weight.shape[1:]
    cap = max(2 * tok // n_sp, 16)
    kw, kn = broad_key_lift.shape[1], slim_key_lift.shape[1]
    heads_w, heads_n = kw // PLAIN_WIDE, kn // PLAIN_SLIM
    keys = n_sp * tok
    slots = n_sp * cap
    blk = min(slots, 256)

    freq = (1.0 / ROPE_BASE ** (np.arange(0, ROPE, 2).astype(np.float32) / np.float32(ROPE))).astype(np.float32)
    freq = np.tile(freq.astype(np.float64), LANES // (ROPE // 2))[None, :]
    base = (np.arange(n_sp) * tok)[:, None] * freq
    local = np.arange(tok)[:, None] * freq
    base_t = jnp.asarray(np.stack([np.cos(base), np.sin(base)]).astype(np.float32))
    local_t = jnp.asarray(np.stack([np.cos(local), np.sin(local)]).astype(np.float32))
    pair = expert_pair.astype(F32)
    meta = jnp.stack([
        group_route.astype(F32), pair[:, 0], pair[:, 1], group_prob, expert_prob[:, 0], expert_prob[:, 1],
        group_prob, group_prob,
    ])
    vm = pl.BlockSpec(memory_space=pltpu.VMEM)
    hb = pl.BlockSpec(memory_space=pl.ANY)
    dma = pltpu.SemaphoreType.DMA
    scratch = [
        pltpu.VMEM(query_wide.shape, BF16), pltpu.VMEM(query_narrow.shape, BF16),
        pltpu.VMEM(latent.shape, BF16), pltpu.VMEM(rope_key.shape, BF16),
        pltpu.VMEM((rank, 2 * kw + 2 * kn), BF16),
        pltpu.VMEM((kw + kn, width), BF16),
        pltpu.VMEM((tok, quarter), BF16),
        pltpu.VMEM((experts, width, 2 * ff), BF16),
        pltpu.VMEM((experts * ff, width), BF16),
        pltpu.VMEM((n_tp, tok // n_tp, rank + LANES), BF16),
        pltpu.VMEM((n_sp, n_tp, tok // n_tp, rank + LANES), BF16),
        pltpu.VMEM((keys, heads_w * 256 + heads_n * 128), BF16),
        pltpu.VMEM((keys, kw + kn), BF16),
        pltpu.VMEM((tok, kw + kn), BF16),
        pltpu.VMEM((4, tok, quarter), BF16),
        pltpu.VMEM((3, tok, quarter), BF16),
        pltpu.VMEM((n_sp, cap, quarter), BF16),
        pltpu.VMEM((n_sp, cap, LANES), BF16),
        pltpu.VMEM((n_sp, n_tp, cap, quarter), BF16),
        pltpu.VMEM((n_sp, cap, LANES), BF16),
        pltpu.VMEM((blk, width), BF16),
        pltpu.VMEM((slots, experts * ff), BF16),
        pltpu.VMEM((4, n_sp, cap, quarter), BF16),
        pltpu.VMEM((2, n_sp, cap, quarter), BF16),
        pltpu.VMEM((n_sp, cap, quarter), BF16),
        pltpu.VMEM((n_sp, cap, quarter), BF16),
        pltpu.VMEM((n_sp, cap, quarter), BF16),
        pltpu.VMEM((n_sp, cap, quarter), BF16),
        dma((13 + experts,)), dma((n_sp, 4)), dma((n_sp, 4)), dma((3,)), dma((3,)), dma((n_sp,)), dma((n_sp,)),
        dma((n_sp, 4)), dma((2,)), dma((2,)), dma((n_sp,)), dma((n_sp,)),
    ]
    call = pl.pallas_call(
        functools.partial(kernel, n_sp, n_tp, cap),
        out_shape=jax.ShapeDtypeStruct((tok, quarter), BF16),
        in_specs=[hb, hb, hb, hb, vm, hb, hb, hb, hb, hb, hb, hb, vm, vm, vm, vm, hb, hb, hb],
        out_specs=vm,
        scratch_shapes=scratch,
        compiler_params=pltpu.CompilerParams(
            collective_id=0, has_side_effects=True, vmem_limit_bytes=67043328
        ),
    )
    return call(
        query_wide, query_narrow, latent, rope_key, latent_norm_weight[None, :], broad_key_lift,
        broad_value_lift, slim_key_lift, slim_value_lift, out_wide, out_narrow, resid, ffn_gain[None, :], meta,
        base_t, local_t, gate_weight, up_weight, down_weight,
    )


def solution(mesh):
    sizes = dict(mesh.shape)
    placed = (
        P("sp", "tp"), P("sp", "tp"), P("sp", None), P("sp", None), P(), P(None, "tp"), P(None, "tp"),
        P(None, "tp"), P(None, "tp"), P("tp", None), P("tp", None), P("sp", None), P(), P("sp"),
        P("sp", None), P("sp"), P("sp", None), P("sp", None, None, "tp"), P("sp", None, None, "tp"),
        P("sp", None, "tp", None),
    )
    return jax.shard_map(
        functools.partial(body, sizes["sp"], sizes["tp"]),
        mesh=mesh, in_specs=placed, out_specs=P("sp", "tp"), check_vma=False,
    )
```

time: 181 us -> 66.6 us (0.37)
  waiting for transfers between devices: 78.5 us -> 0 us
  Pallas kernels: 0 us -> 59.8 us
  blocking collectives: 51.6 us -> 0 us
  between operations: 14 us -> 0.01 us
  matrix products: 13.2 us -> 0 us
  other arithmetic: 10.8 us -> 1.34 us
  starting transfers between devices: 5.64 us -> 0 us
    pallas_call x0 -> x1, Pallas kernels: none -> 59.8 us  [body(): call(query_wide, query_narrow, latent, rope_key, latent_norm_weight[None,...]
    psum x1 -> x0, waiting for transfers between devices: 31.1 us -> none  [body(): lax.psum(partial_value.astype(jnp.bfloat16), 'tp').astype(jnp.float32)]
    all_gather x1 -> x0, blocking collectives: 28.3 us -> none  [body(): lax.all_gather(rot_key, 'sp', axis=0, tiled=True)]
    reduce_scatter x1 -> x0, waiting for transfers between devices: 24.9 us -> none  [body(): lax.psum_scatter(partials.astype(jnp.bfloat16), 'tp', scatter_dimension=2...]
    all_to_all x2 -> x0, blocking collectives: 23.3 us -> none  [the longest x1 13.6 us: body(): lax.all_to_all(placed.reshape(groups, capacity, column_rows.shape[1]), 's...]
    all_gather x2 -> x0, waiting for transfers between devices: 13.7 us -> none  [the longest x1 9.58 us: body(): lax.all_gather(latent_rows, 'sp', axis=0, tiled=True)]
    dot_general x15 -> x0, matrix products: 13.2 us -> none  [the longest x4 3.13 us: project(): jnp.dot(latent_rows, weight, preferred_element_type=jnp.float32)]
    all_to_all x1 -> x0, waiting for transfers between devices: 8.74 us -> none  [body(): lax.all_to_all(summed_rows, 'sp', split_axis=0, concat_axis=0, tiled=True)]
  transfers between devices with their start and end apart: 5 -> 0, of which waited for: 5 -> 0; matrix products, arithmetic and copies ran while one was open for 4% -> 0% of each run, Pallas kernels for 0% -> 0%
where the time goes in v1:
time: 66.6 us; the launch traced here: 66.3 us
  Pallas kernels  59.8 us (90%)
  local copies, waits for them, and re-layouts  5.13 us (8%)
  other arithmetic  1.34 us (2%)
    pallas_call x1, Pallas kernels, body(): call(query_wide, query_narrow, latent, rope_key, latent_norm_weight[None,...  59.8 us
    unnamed x2, local copies, waits for them, and re-layouts  3 us
    another operation x2, local copies, waits for them, and re-layouts, body(): jnp.stack([group_route.astype(F32), pair[:, 0], pair[:, 1], group_prob, e...  2.13 us

profile of v1, /device:TPU:0, one launch (start us, length us, event | category | flops | bytes accessed | tf_op | source)
XLA Modules:
  0.0 66.3 jit_solution(12455056172597615529)
XLA Ops:
  0.0 0.7 convert_bitcast_fusion
  0.7 0.7 %convert_element_type.7 = f32[128,2]{0,1:T(2,128)S(1)} convert(s32[128,2]{0,1:T(2,128)} %param.36) | non-fusion elementwise | flops 256 | bytes 2048 | tf_op jit(solution)/shard_map/convert_element_type | solution.py:475
  1.3 0.8 %slice_bitcast_fusion = (f32[1,128]{1,0:T(1,128)S(1)}, f32[1,128]{1,0:T(1,128)S(1)}, f32[1,128]{1,0:T(1,128)S(1)}, f32[1,128]{1,0:T(1,128)S(1)}) fusion(f32[128,2]{0,1:T(2,128)} %param.38, f32[128,2]{0,1:T(2,128)S(1)} %convert_element_type.7), kind=kLoop, calls=%fused_computation | loop fusion | bytes 4096 | tf_op jit(solution)/shard_map/stack;squeeze | solution.py:476
  2.1 1.4 %stack.13.meta = f32[8,128]{1,0:T(8,128)} concatenate(f32[1,128]{1,0:T(1,128)S(1)} %convert_bitcast_fusion, f32[1,128]{1,0:T(1,128)S(1)} %get-tuple-element.9, f32[1,128]{1,0:T(1,128)S(1)} %get-tuple-element.10, f32[1,128]{1,0:T(1,128)} %bitcast.14, f32[1,128]{1,0:T(1,128)S(1)} %get-tuple-element.6, f32[1,128]{1,0:T(1,128)S(1)} %get-tuple-element.5, f32[1,128]{1,0:T(1,128)} %bitcast.15, ...), dimensions={0} | concatenate | bytes 8192 | tf_op jit(solution)/shard_map/stack | solution.py:476
  3.5 1.4 %copy.23.rk_h = bf16[128,64]{1,0:T(8,128)(2,1)} copy(bf16[128,64]{0,1:T(8,128)(2,1)} %param.25) | data formatting | bytes 32768 | tf_op args[3]
  4.9 59.8 %shard_map.208 = bf16[128,512]{1,0:T(8,128)(2,1)} custom-call(bf16[128,384]{1,0:T(8,128)(2,1)} %qw_h.1, bf16[128,256]{1,0:T(8,128)(2,1)} %qn_h.1, bf16[128,512]{1,0:T(8,128)(2,1)} %lat_h.1, bf16[128,64]{1,0:T(8,128)(2,1)} %copy.23.rk_h, f32[1,512]{1,0:T(1,128)} %bitcast.17, bf16[512,256]{1,0:T(8,128)(2,1)} %bk_h.1, bf16[512,256]{1,0:T(8,128)(2,1)} %bv_h.1, ...), custom_call_target="tpu_custom_call" | custom-call | tf_op jit(solution)/shard_map/pallas_call | solution.py:523
  64.7 1.6 %copy.25 = bf16[128,512]{1,0:T(8,128)(2,1)} copy(bf16[128,512]{1,0:T(8,128)(2,1)} %shard_map.208) | data formatting | bytes 262144

commit v2 on v1

--- a/solution.py
+++ b/solution.py
@@ -42,7 +42,7 @@
 
 def kernel(
     n_sp, n_tp, cap,
-    qw_h, qn_h, lat_h, rk_h, lnw, bk_h, bv_h, sk_h, sv_h, ow_h, on_h, res_h, gain, meta,
+    qw_h, qn_h, lat_h, rk_h, lnw, bk_h, bv_h, sk_h, sv_h, ow_h, on_h, res_h, gain, route_r, pair_r, gprob_r, eprob_r,
     base_t, local_t, gate_h, up_h, down_h,
     out_ref,
     qw, qn, lat, rk, lift, wout, res, gu, down,
@@ -125,7 +125,7 @@
         c.wait()
     dup = (lax.broadcasted_iota(jnp.int32, (ROPE, LANES), 0)
            == lax.rem(lax.broadcasted_iota(jnp.int32, (ROPE, LANES), 1), 64)).astype(BF16)
-    rk2 = turn(dot(rk[...], dup), cos, sin).astype(BF16)
+    rk2 = turn(dot_tn(rk[...], dup), cos, sin).astype(BF16)
     x = lat[...].astype(F32)
     rows = (x * lax.rsqrt(jnp.mean(x * x, axis=-1, keepdims=True) + EPSILON) * lnw[...]).astype(BF16)
     own_lat[:, :, 0:rank] = rows.reshape(n_tp, piece, rank)
@@ -140,13 +140,24 @@
             src_ref=src, dst_ref=dst, send_sem=s_sem, recv_sem=r_sem, device_id=dev, device_id_type=MESH
         )
 
+    odd = lax.rem(me, 2)
+    other = me + 1 - 2 * odd
+
     def lat_sp(dest):
         return copy(own_lat.at[j], lat_all.at[me, j], snd.at[dest, 0], rcv_a.at[me, 0], (dest, j))
 
-    loop(me + 1, n_sp, lambda d: lat_sp(d).start())
-
-    meta_v = meta[...]
-    route = meta_v[0:1, :]
+    def lat_pass(s):
+        return copy(lat_all.at[s, j], lat_all.at[s, j], snd.at[s, 0], rcv_a.at[s, 0], (other, j))
+
+    later = lax.div(n_sp - 1 - me, 2)
+
+    @pl.when(odd == 0)
+    def _():
+        lat_sp(other).start()
+
+    loop(0, later, lambda i: lat_sp(me + 2 + 2 * i).start())
+
+    route = route_r[...].astype(F32)
     gcol = lax.broadcasted_iota(jnp.int32, (max(n_sp, 8), tok), 0).astype(F32)
     member = (gcol == route).astype(F32)
     upper = (lax.broadcasted_iota(jnp.int32, (tok, tok), 0)
@@ -157,11 +168,12 @@
     slot_iota = lax.broadcasted_iota(jnp.int32, (slots, tok), 0).astype(F32)
     place = (slot_iota == slot_row).astype(BF16)
     eiota = lax.broadcasted_iota(jnp.int32, (LANES, tok), 0).astype(F32)
-    total = meta_v[4:5, :] + meta_v[5:6, :]
+    pair = pair_r[...].astype(F32)
+    total = eprob_r[0:1, :] + eprob_r[1:2, :]
     combine = jnp.zeros((LANES, tok), F32)
     for k in range(2):
-        share = meta_v[3:4, :] * meta_v[4 + k:5 + k, :] / total
-        combine = combine + jnp.where(eiota == meta_v[1 + k:2 + k, :], share, 0.0)
+        share = gprob_r[...] * eprob_r[k:k + 1, :] / total
+        combine = combine + jnp.where(eiota == pair[k:k + 1, :], share, 0.0)
     cs_v = dot_nt(place, combine.astype(BF16)).astype(BF16).reshape(n_sp, cap, LANES)
     cs[...] = cs_v
 
@@ -238,27 +250,38 @@
             kbuf[at, off + h * 128:off + (h + 1) * 128] = mixed
         vbuf[at, kw:] = kv[:, 2 * kw + kn:]
 
-    def a1(i):
-        s = me - 1 - i
+    def a1(i, s):
         arrived(lat_all, s, 0, rcv_a)
         gather(lat_all, s, 2, rcv_a).start()
         gather(lat_all, s, 1, rcv_a).start()
 
-    def a2(i):
-        s = me - 1 - i
+        @pl.when(lax.rem(i, 2) == 0)
+        def _():
+            lat_pass(s).start()
+
+    def a2(i, s):
         arrived(lat_all, s, 2, rcv_a)
         gather(lat_all, s, 3, rcv_a).start()
 
-    def a3(i):
-        s = me - 1 - i
+    def a3(i, s):
         arrived(lat_all, s, 1, rcv_a)
         arrived(lat_all, s, 3, rcv_a)
         expand(s)
 
+    steps = me + odd
+
+    def a_step(t):
+        for lag, fn in ((0, a1), (2, a2), (3, a3)):
+            i = t - lag
+            i0 = jnp.maximum(i, 0)
+            s = me - 2 - i0 + 2 * lax.rem(i0, 2)
+
+            @pl.when((i >= 0) & (i < steps) & (s >= 0))
+            def _():
+                fn(i0, s)
+
     expand(me)
-    loop(0, me, a1)
-    loop(0, me, a2)
-    loop(0, me, a3)
+    loop(0, steps + 3, a_step)
 
     keys = n_sp * tok
     chunk = min(keys, 1024)
@@ -302,18 +325,28 @@
         c.wait()
 
     def swap_b(r):
-        return copy(part.at[r], part_in.at[r - 1], snd_b.at[r - 1], rcv_b.at[r - 1], (me, rel[r]))
-
-    for r in (2, 3, 1, 0):
+        slot, dest = {1: (0, j1), 2: (2, j2), 3: (1, j1)}[r]
+        return copy(part.at[r], part_in.at[slot], snd_b.at[slot], rcv_b.at[slot], (me, dest))
+
+    def project(r):
         cols = pl.ds(pl.multiple_of(rel[r] * quarter, quarter), quarter)
-        y = dot(att[...], wout[:, cols])
-        if r == 0:
-            mine = y.astype(BF16).astype(F32)
-        else:
-            part[r] = y.astype(BF16)
-            swap_b(r).start()
-
-    loop(me + 1, n_sp, lambda d: lat_sp(d).wait_send())
+        return dot(att[...], wout[:, cols])
+
+    for r in (3, 1):
+        part[r] = project(r).astype(BF16)
+        swap_b(r).start()
+    crossing = project(2)
+    swap_b(3).wait_recv()
+    part[2] = (crossing + part_in[1].astype(F32)).astype(BF16)
+    swap_b(2).start()
+    mine = project(0)
+
+    @pl.when(odd == 0)
+    def _():
+        lat_sp(other).wait_send()
+
+    loop(0, later, lambda i: lat_sp(me + 2 + 2 * i).wait_send())
+    loop(0, lax.div(me, 2), lambda i: lat_pass(me - 2 - 2 * i).wait_send())
 
     def a_done(s):
         for r in (1, 2, 3):
@@ -321,9 +354,9 @@
 
     loop(0, me, a_done)
 
-    for r in (1, 2, 3):
-        swap_b(r).wait_recv()
-        mine = mine + part_in[r - 1].astype(F32)
+    swap_b(1).wait_recv()
+    swap_b(2).wait_recv()
+    mine = mine + part_in[0].astype(F32) + part_in[2].astype(F32)
     stream = (res[...].astype(F32) + mine).astype(BF16)
 
     xs[...] = dot(place, stream).astype(BF16).reshape(n_sp, cap, quarter)
@@ -336,16 +369,13 @@
 
     others(lambda d: rows_sp(d).start())
 
+    def source(i):
+        return lax.rem(me - i + n_sp, n_sp)
+
     def c1(s):
         gather(rx, s, 2, rcv_c).start()
         gather(rx, s, 1, rcv_c).start()
 
-    c1(me)
-
-    def c1w(s):
-        arrived(rx, s, 0, rcv_c)
-        c1(s)
-
     def c2(s):
         arrived(rx, s, 2, rcv_c)
         gather(rx, s, 3, rcv_c).start()
@@ -354,14 +384,23 @@
         arrived(rx, s, 1, rcv_c)
         arrived(rx, s, 3, rcv_c)
 
-    others(c1w)
-    c2(me)
-    others(c2)
+    c1(me)
+
+    def c_step(t):
+        @pl.when(t < n_sp)
+        def _():
+            arrived(rx, source(t), 0, rcv_c)
+            c1(source(t))
+
+        @pl.when(t >= 2)
+        def _():
+            c2(source(jnp.maximum(t - 2, 0)))
+
+    loop(1, n_sp + 2, c_step)
     for c in weights:
         c.wait()
     others(lambda s: copy(cs.at[s], comb.at[s], snd_k.at[s], rcv_k.at[s], (s, j)).wait_recv())
-    c3(me)
-    others(c3)
+    loop(0, n_sp, lambda i: c3(source(i)))
 
     blk = min(slots, 256)
     per = blk // cap
@@ -384,15 +423,17 @@
     def swap_d(i):
         return copy(pd.at[3 if i else 1], d1.at[i], snd_d.at[i], rcv_d1.at[i], (me, j1))
 
-    for r in (3, 1, 2, 0):
+    def product(r):
         cols = pl.ds(pl.multiple_of(rel[r] * quarter, quarter), quarter)
         for b in range(slots // blk):
             y = dot(hid[b * blk:(b + 1) * blk], down[:, cols]).astype(BF16)
             pd[r, b * per:(b + 1) * per] = y.reshape(per, cap, quarter)
-        if r == 3:
-            swap_d(1).start()
-        if r == 1:
-            swap_d(0).start()
+
+    product(3)
+    swap_d(1).start()
+    product(1)
+    swap_d(0).start()
+    product(2)
 
     others(lambda d: rows_sp(d).wait_send())
 
@@ -419,6 +460,7 @@
 
     others(d_pair)
     d_pair(me)
+    product(0)
     swap_d(0).wait_recv()
 
     def summed(s):
@@ -472,17 +514,12 @@
     local = np.arange(tok)[:, None] * freq
     base_t = jnp.asarray(np.stack([np.cos(base), np.sin(base)]).astype(np.float32))
     local_t = jnp.asarray(np.stack([np.cos(local), np.sin(local)]).astype(np.float32))
-    pair = expert_pair.astype(F32)
-    meta = jnp.stack([
-        group_route.astype(F32), pair[:, 0], pair[:, 1], group_prob, expert_prob[:, 0], expert_prob[:, 1],
-        group_prob, group_prob,
-    ])
     vm = pl.BlockSpec(memory_space=pltpu.VMEM)
     hb = pl.BlockSpec(memory_space=pl.ANY)
     dma = pltpu.SemaphoreType.DMA
     scratch = [
         pltpu.VMEM(query_wide.shape, BF16), pltpu.VMEM(query_narrow.shape, BF16),
-        pltpu.VMEM(latent.shape, BF16), pltpu.VMEM(rope_key.shape, BF16),
+        pltpu.VMEM(latent.shape, BF16), pltpu.VMEM(rope_key.shape[::-1], BF16),
         pltpu.VMEM((rank, 2 * kw + 2 * kn), BF16),
         pltpu.VMEM((kw + kn, width), BF16),
         pltpu.VMEM((tok, quarter), BF16),
@@ -513,7 +550,7 @@
     call = pl.pallas_call(
         functools.partial(kernel, n_sp, n_tp, cap),
         out_shape=jax.ShapeDtypeStruct((tok, quarter), BF16),
-        in_specs=[hb, hb, hb, hb, vm, hb, hb, hb, hb, hb, hb, hb, vm, vm, vm, vm, hb, hb, hb],
+        in_specs=[hb, hb, hb, hb, vm, hb, hb, hb, hb, hb, hb, hb, vm, vm, vm, vm, vm, vm, vm, hb, hb, hb],
         out_specs=vm,
         scratch_shapes=scratch,
         compiler_params=pltpu.CompilerParams(
@@ -521,9 +558,9 @@
         ),
     )
     return call(
-        query_wide, query_narrow, latent, rope_key, latent_norm_weight[None, :], broad_key_lift,
-        broad_value_lift, slim_key_lift, slim_value_lift, out_wide, out_narrow, resid, ffn_gain[None, :], meta,
-        base_t, local_t, gate_weight, up_weight, down_weight,
+        query_wide, query_narrow, latent, rope_key.T, latent_norm_weight[None, :], broad_key_lift,
+        broad_value_lift, slim_key_lift, slim_value_lift, out_wide, out_narrow, resid, ffn_gain[None, :],
+        group_route[None, :], expert_pair.T, group_prob[None, :], expert_prob.T, base_t, local_t, gate_weight, up_weight, down_weight,
     )
 
 

time: 66.6 us -> 61 us (0.916)
  local copies, waits for them, and re-layouts: 5.13 us -> 1.57 us
  other arithmetic: 1.34 us -> 0 us
    another operation x2 -> x0, local copies, waits for them, and re-layouts: 2.13 us -> none  [body(): jnp.stack([group_route.astype(F32), pair[:, 0], pair[:, 1], group_prob, e...]
    unnamed x2 -> x1, local copies, waits for them, and re-layouts: 3 us -> 1.57 us
    convert_element_type x1 -> x0, other arithmetic: 0.68 us -> none  [body(): pair = expert_pair.astype(F32)]
where the time goes in v2:
time: 61 us; the launch traced here: 60.8 us
  Pallas kernels  59.3 us (97%)
  local copies, waits for them, and re-layouts  1.57 us (3%)
    pallas_call x1, Pallas kernels, body(): call(query_wide, query_narrow, latent, rope_key.T, latent_norm_weight[Non...  59.3 us
    unnamed x1, local copies, waits for them, and re-layouts  1.57 us

profile of v2, /device:TPU:0, one launch (start us, length us, event | category | flops | bytes accessed | tf_op | source)
XLA Modules:
  0.0 60.8 jit_solution(9941365046951970273)
XLA Ops:
  0.0 59.3 %shard_map.208 = bf16[128,512]{1,0:T(8,128)(2,1)} custom-call(bf16[128,384]{1,0:T(8,128)(2,1)} %qw_h.1, bf16[128,256]{1,0:T(8,128)(2,1)} %qn_h.1, bf16[128,512]{1,0:T(8,128)(2,1)} %lat_h.1, bf16[64,128]{1,0:T(8,128)(2,1)} %bitcast.7, f32[1,512]{1,0:T(1,128)} %bitcast.9, bf16[512,256]{1,0:T(8,128)(2,1)} %bk_h.1, bf16[512,256]{1,0:T(8,128)(2,1)} %bv_h.1, ...), custom_call_target="tpu_custom_call" | custom-call | tf_op jit(solution)/shard_map/pallas_call | solution.py:560
  59.3 1.6 %copy.24 = bf16[128,512]{1,0:T(8,128)(2,1)} copy(bf16[128,512]{1,0:T(8,128)(2,1)} %shard_map.208) | data formatting | bytes 262144
